TPU v7x, 32 devices: a whole 2x2x4 slice. The times are simulated.
32 devices in a mesh: sp: 8 (over z, y), tp: 4 (over x, core).
Axes of the slice: x: 2, y: 2, z: 4, core: 2. Of those that a mesh axis runs over, the one named last changes fastest.
Arguments:
- residual: bfloat16 [3072, 2048], P('sp'), may hold values from -50 to 50
- queries_a: bfloat16 [3072, 512], P('sp', 'tp'), may hold values from -50 to 50
- keys_a: bfloat16 [3072, 512], P('sp', 'tp'), may hold values from -9 to 9
- values_a: bfloat16 [3072, 512], P('sp', 'tp'), may hold values from -6 to 6
- queries_b: bfloat16 [3072, 1024], P('sp', 'tp'), may hold values from -50 to 50
- keys_b: bfloat16 [3072, 1024], P('sp', 'tp'), may hold values from -9 to 9
- values_b: bfloat16 [3072, 512], P('sp', 'tp'), may hold values from -6 to 6
- mix_lambda: float32 [2, 4], P(None, 'tp'), may hold values from 0.3 to 0.8
- head_gain: float32 [2, 128], replicated, may hold values from 0.1 to 1.9
- out_a: bfloat16 [512, 2048], P('tp'), may hold values from -0.1875 to 0.1875
- out_b: bfloat16 [512, 2048], P('tp'), may hold values from -0.1875 to 0.1875
- norm_gain: float32 [2048], replicated, may hold values from 0.1 to 1.9
- w_gate: bfloat16 [2048, 5632], P('sp', 'tp'), may hold values from -0.125 to 0.125
- w_up: bfloat16 [2048, 5632], P('sp', 'tp'), may hold values from -0.125 to 0.125
- w_down: bfloat16 [5632, 2048], P('tp', 'sp'), may hold values from -0.21875 to 0.21875
Outputs:
- layer_out: bfloat16 [3072, 2048], P('sp', 'tp')
All inputs are finite; a program needn't handle non-finite values.
Results may differ from a plain program's by a relative error of at most 0.0085.
Values may be sent and summed in bfloat16 or wider, within the bound.
A program may use at most 256 MiB of HBM per device.

v0:
```python
import functools
import math

import jax
import jax.numpy as jnp
from jax import lax
from jax.experimental import pallas as pl
from jax.experimental.pallas import tpu as pltpu
from jax.sharding import PartitionSpec as P

eps_norm = 1e-06
head_scale = 0.8
MESH = pl.DeviceIdType.MESH
CHUNKS = 2
CUTS = 3
NT = (((1,), (1,)), ((), ()))


def ring_to_sp(pos, n):
    late = pos // (n // 2)
    return (1 - late) * 2 * pos + late * (2 * (n - 1 - pos) + 1)


def sp_to_ring(index, n):
    odd = index % 2
    return (1 - odd) * (index // 2) + odd * (n - 1 - (index - odd) // 2)


def flip(index, bit):
    return index + bit - 2 * bit * ((index // bit) % 2)


def flip_all(index, mask):
    bit = 1
    while bit <= mask:
        if mask & bit:
            index = flip(index, bit)
        bit *= 2
    return index


def kernel(
    n, tp, residual, qa, ka, va, qb, kb, vb, lam, gain, oa, ob, ngain, wg, wu, wd, out,
    kv_all, wg_turn, wu_turn, wg_all, wu_all, wd_all, out_all, heads_all, summed, normed, hidden, channel, sbuf,
    rbuf, tbuf, ubuf, mine, local_sem, ring_send, ring_recv, cube_send, cube_recv, out_send, out_recv, head_send,
    head_recv, swap_sem, norm_send, norm_recv, red_send, red_recv,
):
    rows, width = residual.shape
    heads = lam.shape[1]
    sa, sb = qa.shape[1] // (2 * heads), qb.shape[1] // (2 * heads)
    vd = va.shape[1] // heads
    hv = heads * vd
    total = n * rows
    block = math.gcd(rows, 1 << min(7, ((1 << 19) // total).bit_length() - 1))
    nb = rows // block
    share = width // tp
    depth, units = wg.shape
    half = units // 2
    sp_me, tp_me = lax.axis_index("sp"), lax.axis_index("tp")
    pos = sp_to_ring(sp_me, n)
    targets = (ring_to_sp((pos + 1) % n, n), ring_to_sp((pos + n - 1) % n, n))
    peers = [(tp_me + k) % tp for k in range(1, tp)]
    pair = n // 4
    side = (sp_me // pair) % 2
    mate = flip(sp_me, pair)
    bits = [pair, n // 2]
    while bits[-1 if len(bits) > 2 else 0] > 1:
        bits.append(bits[-1] // 2 if len(bits) > 2 else pair // 2)

    ck, cv = ka.shape[1], ka.shape[1] + kb.shape[1]
    own_kv = kv_all.at[sp_me]
    own = [
        (ka, own_kv.at[:, pl.ds(0, ck)]),
        (kb, own_kv.at[:, pl.ds(ck, kb.shape[1])]),
        (va, own_kv.at[:, pl.ds(cv, hv)]),
        (vb, own_kv.at[:, pl.ds(cv + hv, hv)]),
        (wd.at[pl.ds(pl.multiple_of(side * half, half), half)], wd_all.at[sp_me]),
        (oa, out_all.at[tp_me, pl.ds(0, hv)]),
        (ob, out_all.at[tp_me, pl.ds(hv, hv)]),
    ]
    copies = [pltpu.make_async_copy(s, d, local_sem.at[i]) for i, (s, d) in enumerate(own)]
    for c in copies:
        c.start()

    barrier = pltpu.get_barrier_semaphore()
    for target in list(targets) + [flip(sp_me, bit) for bit in bits]:
        pl.semaphore_signal(barrier, inc=1, device_id={"sp": target}, device_id_type=MESH)
    for peer in peers:
        pl.semaphore_signal(barrier, inc=1, device_id={"tp": peer}, device_id_type=MESH)
    for c in copies:
        c.wait()
    pl.semaphore_wait(barrier, 2 + len(bits) + len(peers))

    def piece(c, d, t, dist):
        owner = ring_to_sp((pos + n - dist) % n if d == 0 else (pos + dist) % n, n)
        part = rows // (2 * CHUNKS)
        view = kv_all.at[owner, pl.ds((d * CHUNKS + c) * part, part)]
        return pltpu.make_async_remote_copy(
            src_ref=view, dst_ref=view,
            send_sem=ring_send.at[c, d, t], recv_sem=ring_recv.at[c, d, t],
            device_id={"sp": targets[d]}, device_id_type=MESH,
        )

    for c in range(CHUNKS):
        for d in range(2):
            piece(c, d, 0, 0).start()

    tp_bits = []
    while (tp >> (len(tp_bits) + 1)) > 0:
        tp_bits.append(tp >> (len(tp_bits) + 1))
    tp_order, tp_came = [0], {}
    for k, bit in enumerate(tp_bits):
        for held in list(tp_order):
            tp_came[held | bit] = (held, k)
            tp_order.append(held | bit)

    def tp_copy(gather, held, k, arriving):
        view, first, sends, recvs = gather
        mask = held | tp_bits[k]
        dst = view(flip_all(tp_me, mask if arriving else held))
        return pltpu.make_async_remote_copy(
            src_ref=first if first is not None and held == 0 and not arriving else dst, dst_ref=dst,
            send_sem=sends.at[mask - 1], recv_sem=recvs.at[mask - 1],
            device_id={"tp": flip(tp_me, tp_bits[k])}, device_id_type=MESH,
        )

    def tp_forward(gather, mask):
        for k in range(tp_came[mask][1] + 1 if mask else 0, len(tp_bits)):
            tp_copy(gather, mask, k, False).start()

    def tp_arrive(gather, masks):
        for mask in masks:
            held, k = tp_came[mask]
            tp_copy(gather, held, k, True).wait_recv()
            tp_forward(gather, mask)

    def tp_drain(gather):
        for mask in tp_order[1:]:
            held, k = tp_came[mask]
            tp_copy(gather, held, k, False).wait_send()

    out_gather = (lambda slot: out_all.at[slot], None, out_send, out_recv)
    head_gather = (lambda slot: heads_all.at[slot], mine, head_send, head_recv)
    norm_gather = (lambda slot: normed.at[1 - side, slot], None, norm_send, norm_recv)
    tp_forward(out_gather, 0)

    tile = math.gcd(units, 128)

    def turn(i):
        at = pl.ds(pl.multiple_of(i * tile, tile), tile)
        wg_turn[at, :] = wg[:, at].T
        wu_turn[at, :] = wu[:, at].T

    turns = units // tile
    per = -(-turns // (n - 1))

    def circulate(t, _):
        for c in range(CHUNKS):
            for d in range(2):
                piece(c, d, t, t + 1).wait_recv()

                @pl.when(t + 1 < n - 1)
                def _():
                    piece(c, d, t + 1, t + 1).start()

        for k in range(per):
            @pl.when(t * per + k < turns)
            def _():
                turn(t * per + k)

        return 0

    lax.fori_loop(0, n - 1, circulate, 0)
    wg_all[sp_me] = wg_turn[pl.ds(pl.multiple_of(side * half, half), half), :]
    wu_all[sp_me] = wu_turn[pl.ds(pl.multiple_of(side * half, half), half), :]

    gathered = (wg_all, wu_all, wd_all)
    whole = (wg_turn, wu_turn, wd)

    def cube(a, held, k, arriving):
        mask = held | bits[k]
        owner = flip_all(sp_me, mask if arriving else held)
        dst = gathered[a].at[owner]
        src = dst
        if k == 0 and not arriving:
            src = whole[a].at[pl.ds(pl.multiple_of((1 - side) * half, half), half)]
        return pltpu.make_async_remote_copy(
            src_ref=src, dst_ref=dst,
            send_sem=cube_send.at[a, mask], recv_sem=cube_recv.at[a, mask],
            device_id={"sp": flip(sp_me, bits[k])}, device_id_type=MESH,
        )

    order = [0]
    came = {}
    for k, bit in enumerate(bits):
        for held in list(order):
            came[held | bit] = (held, k)
            order.append(held | bit)

    def forward(a, mask, least=0, most=len(bits)):
        first = came[mask][1] + 1 if mask else 0
        for k in range(max(first, least), most):
            cube(a, mask, k, False).start()

    def arrive(a, mask):
        held, k = came[mask]
        cube(a, held, k, True).wait_recv()
        forward(a, mask)

    forward(0, 0)
    forward(1, 0)
    forward(2, 0, least=2)
    events = []
    for k in range(len(bits)):
        for a in range(3):
            for mask in order[1:]:
                if came[mask][1] == k:
                    events.append((a, mask))

    def take(chosen):
        for a, mask in chosen:
            arrive(a, mask)
            events.remove((a, mask))

    def attend(group, r):
        queries = qa if group == 0 else qb
        size = sa if group == 0 else sb
        base = 0 if group == 0 else ck
        factor = size ** (-0.5) * math.log2(math.e)
        at = pl.ds(pl.multiple_of(r * block, block), block)
        for h in range(heads):
            start = 2 * h * size
            query = queries[at, start : start + 2 * size]
            value = kv_all[:, :, cv + group * hv + h * vd : cv + group * hv + (h + 1) * vd].reshape(total, vd)
            lanes = lax.broadcasted_iota(jnp.int32, query.shape, 1)
            ratios = []
            for j in range(2):
                if size % 128 == 0:
                    q = query[:, j * size : (j + 1) * size]
                    low = base + start + j * size
                    key = kv_all[:, :, low : low + size].reshape(total, size)
                else:
                    q = jnp.where(lanes // size == j, query, jnp.zeros_like(query))
                    low = base + start
                    key = kv_all[:, :, low : low + 2 * size].reshape(total, 2 * size)
                scores = lax.dot_general(q, key, NT, preferred_element_type=jnp.float32)
                peak = jnp.max(scores, axis=1, keepdims=True)
                weights = jnp.exp2((scores - peak) * factor)
                denom = jnp.sum(weights, axis=1, keepdims=True)
                numer = jnp.dot(weights.astype(jnp.bfloat16), value, preferred_element_type=jnp.float32)
                ratios.append(numer / denom)
            mixed = ratios[0] - lam[group, h] * ratios[1]
            inverse = lax.rsqrt(jnp.mean(mixed * mixed, axis=-1, keepdims=True) + eps_norm)
            result = mixed * inverse * gain[group : group + 1, :] * head_scale
            col = group * hv + h * vd
            mine[at, col : col + vd] = result.astype(jnp.bfloat16)

    early = [(a, mask) for a, mask in events if a < 2 and came[mask][1] < 2]
    portion = -(-len(early) // (2 * CUTS))
    cuts = [nb * i // CUTS for i in range(CUTS + 1)]
    for group in range(2):
        for i in range(CUTS):
            def body(r, _, group=group):
                attend(group, r)
                return 0

            lax.fori_loop(cuts[i], cuts[i + 1], body, 0)
            take(early[:portion])
            early = early[portion:]
            if group == 0 and i == 0:
                tp_arrive(out_gather, tp_order[1:-1])
            if group == 0 and i == 1:
                tp_arrive(out_gather, tp_order[-1:])

    tp_forward(head_gather, 0)
    tp_arrive(head_gather, tp_order[1:])
    heads_all[tp_me] = mine[...]

    def project(r, _):
        at = pl.ds(pl.multiple_of(r * block, block), block)
        acc = residual[at, :].astype(jnp.float32)
        for d in range(tp):
            acc = acc + jnp.dot(heads_all[d, at, :], out_all[d], preferred_element_type=jnp.float32)
        inverse = lax.rsqrt(jnp.mean(acc * acc, axis=-1, keepdims=True) + eps_norm)
        scaled = (acc * inverse * ngain[...]).astype(jnp.bfloat16)
        for d in range(tp):
            normed[side, d, at, :] = scaled[:, d * share : (d + 1) * share]
            summed[d, at, :] = acc[:, d * share : (d + 1) * share].astype(summed.dtype)
        return 0

    lax.fori_loop(0, nb, project, 0)

    def swap(arriving):
        there = 1 - side if arriving else side
        view = normed.at[there, tp_me]
        return pltpu.make_async_remote_copy(
            src_ref=view, dst_ref=view, send_sem=swap_sem.at[0], recv_sem=swap_sem.at[1],
            device_id={"sp": mate}, device_id_type=MESH,
        )

    swap(False).start()
    forward(2, 0, most=2)
    take([e for e in events if e[0] == 2 and came[e[1]][1] == 0])
    swap(True).wait_recv()
    tp_forward(norm_gather, 0)
    tp_arrive(norm_gather, tp_order[1:-1])
    take([e for e in events if e[0] < 2])

    step_cols = share // depth

    def feed(where):
        gate = jnp.zeros((rows, half), jnp.float32)
        upward = jnp.zeros((rows, half), jnp.float32)
        for s in range(n):
            low = (s % step_cols) * depth
            x = normed[where, s // step_cols, :, low : low + depth]
            gate = gate + lax.dot_general(x, wg_all[s], NT, preferred_element_type=jnp.float32)
            upward = upward + lax.dot_general(x, wu_all[s], NT, preferred_element_type=jnp.float32)
        hidden[where] = (gate / (1.0 + jnp.exp(-gate)) * upward).astype(jnp.bfloat16)

    def feed_one(i, _):
        @pl.when(i == 1)
        def _():
            tp_arrive(norm_gather, tp_order[-1:])

        feed((side + i) % 2)
        return 0

    lax.fori_loop(0, 2, feed_one, 0)
    take(list(events))

    cols = wd_all.shape[2]
    ratio = share // cols
    low_bit = tp_me % 2

    def block_sum(d, where):
        return [
            jnp.dot(hidden[where], wd_all[d * ratio + s], preferred_element_type=jnp.float32)
            for s in range(ratio)
        ]

    used, pending = 0, []

    def send(src, dst, **target):
        nonlocal used
        copy = pltpu.make_async_remote_copy(
            src_ref=src, dst_ref=dst, send_sem=red_send.at[used], recv_sem=red_recv.at[used],
            device_id=target, device_id_type=MESH,
        )
        copy.start()
        pending.append(copy)
        used += 1

    for i in range(2):
        for m in range(tp // 2):
            d = 2 * m + (1 - low_bit if i == 0 else low_bit)
            for where in range(2):
                for s, value in enumerate(block_sum(d, where)):
                    if i == 0:
                        sbuf[2 * m + where, :, s * cols : (s + 1) * cols] = value.astype(jnp.bfloat16)
                    else:
                        channel[2 * m + where, :, s * cols : (s + 1) * cols] = value
                if i == 0:
                    send(sbuf.at[2 * m + where], rbuf.at[2 * m + where], tp=flip(tp_me, 1))
    for m in range(tp):
        pending[m].wait_recv()
        channel[m] = channel[m] + rbuf[m].astype(jnp.float32)

    strip = rows // 2
    sent = 0
    states = [{"bit": 2, "mate": False}, {"bit": 2, "mate": False}]
    stages = len(tp_bits)
    for stage in range(stages):
        batch = []
        for lower in range(2):
            state = states[lower]
            at = pl.ds(lower * strip, strip)
            bit = state["bit"]
            moves = []
            if stage == (0 if lower else stages - 1):
                for q in range(tp // bit):
                    d = (tp_me % bit + bit * q) // 2
                    moves.append((2 * d + 1 - side, 2 * d + side))
                state["mate"] = True
                target = {"sp": mate}
            else:
                flag = (tp_me // bit) % 2
                for m in range(tp // (2 * bit)):
                    give = (tp_me % bit + bit * (1 - flag) + 2 * bit * m) // 2
                    keep = (tp_me % bit + bit * flag + 2 * bit * m) // 2
                    for where in [side] if state["mate"] else [1 - side, side]:
                        moves.append((2 * give + where, 2 * keep + where))
                state["bit"] = 2 * bit
                target = {"tp": flip(tp_me, bit)}
            for give, keep in moves:
                tbuf[sent] = channel[give, at, :].astype(jnp.bfloat16)
                batch.append((used, sent, keep, at))
                send(tbuf.at[sent], ubuf.at[sent], **target)
                sent += 1
        for index, slot, keep, at in batch:
            pending[index].wait_recv()
            channel[keep, at, :] = channel[keep, at, :] + ubuf[slot].astype(jnp.float32)
    final = channel[2 * (tp_me // 2) + side]
    out[...] = (summed[tp_me] + 0.5 * final).astype(jnp.bfloat16)

    for copy in pending:
        copy.wait_send()
    swap(False).wait_send()
    for gather in (out_gather, head_gather, norm_gather):
        tp_drain(gather)
    for a in range(3):
        for mask in order[1:]:
            held, k = came[mask]
            cube(a, held, k, False).wait_send()

    def drain(t, _):
        for c in range(CHUNKS):
            for d in range(2):
                piece(c, d, t, t).wait_send()
        return 0

    lax.fori_loop(0, n - 1, drain, 0)


def local(
    n, tp, residual, queries_a, keys_a, values_a, queries_b, keys_b, values_b, mix_lambda, head_gain,
    out_a, out_b, norm_gain, w_gate, w_up, w_down,
):
    rows, width = residual.shape
    share = width // tp
    units = w_gate.shape[1]
    hv = out_a.shape[0]
    span = keys_a.shape[1] + keys_b.shape[1] + values_a.shape[1] + values_b.shape[1]
    vmem, anywhere = pl.BlockSpec(memory_space=pltpu.VMEM), pl.BlockSpec(memory_space=pl.ANY)
    smem = pl.BlockSpec(memory_space=pltpu.SMEM)
    bf16, f32 = jnp.bfloat16, jnp.float32
    dma = pltpu.SemaphoreType.DMA
    return pl.pallas_call(
        functools.partial(kernel, n, tp),
        out_shape=jax.ShapeDtypeStruct((rows, share), bf16),
        in_specs=[
            vmem, vmem, anywhere, anywhere, vmem, anywhere, anywhere, smem, vmem,
            anywhere, anywhere, vmem, vmem, vmem, anywhere,
        ],
        out_specs=vmem,
        scratch_shapes=[
            pltpu.VMEM((n, rows, span), bf16),
            pltpu.VMEM((units, w_gate.shape[0]), bf16),
            pltpu.VMEM((units, w_gate.shape[0]), bf16),
            pltpu.VMEM((n, units // 2, w_gate.shape[0]), bf16),
            pltpu.VMEM((n, units // 2, w_gate.shape[0]), bf16),
            pltpu.VMEM((n, units // 2, w_down.shape[1]), bf16),
            pltpu.VMEM((tp, 2 * hv, width), bf16),
            pltpu.VMEM((tp, rows, 2 * hv), bf16),
            pltpu.VMEM((tp, rows, share), f32),
            pltpu.VMEM((2, tp, rows, share), bf16),
            pltpu.VMEM((2, rows, units // 2), bf16),
            pltpu.VMEM((tp, rows, share), f32),
            pltpu.VMEM((tp, rows, share), bf16),
            pltpu.VMEM((tp, rows, share), bf16),
            pltpu.VMEM((2 * (tp - 1), rows // 2, share), bf16),
            pltpu.VMEM((2 * (tp - 1), rows // 2, share), bf16),
            pltpu.VMEM((rows, 2 * hv), bf16),
            dma((7,)),
            dma((CHUNKS, 2, n - 1)),
            dma((CHUNKS, 2, n - 1)),
            dma((3, n)),
            dma((3, n)),
            dma((tp - 1,)),
            dma((tp - 1,)),
            dma((tp - 1,)),
            dma((tp - 1,)),
            dma((2,)),
            dma((tp - 1,)),
            dma((tp - 1,)),
            dma((3 * tp - 2,)),
            dma((3 * tp - 2,)),
        ],
        compiler_params=pltpu.CompilerParams(
            collective_id=0, has_side_effects=True, vmem_limit_bytes=63 * 1024 * 1024
        ),
        name="layer",
    )(
        residual, queries_a, keys_a, values_a, queries_b, keys_b, values_b, mix_lambda, head_gain,
        out_a, out_b, norm_gain.reshape(1, -1), w_gate, w_up, w_down,
    )


def solution(mesh):
    in_specs = (
        P("sp", None),
        P("sp", "tp"),
        P("sp", "tp"),
        P("sp", "tp"),
        P("sp", "tp"),
        P("sp", "tp"),
        P("sp", "tp"),
        P(None, "tp"),
        P(),
        P("tp", None),
        P("tp", None),
        P(),
        P("sp", "tp"),
        P("sp", "tp"),
        P("tp", "sp"),
    )
    body = functools.partial(local, mesh.shape["sp"], mesh.shape["tp"])
    return jax.shard_map(body, mesh=mesh, in_specs=in_specs, out_specs=P("sp", "tp"), check_vma=False)
```

profile of v0, /device:TPU:0, one launch (start us, length us, event | category | flops | bytes accessed | tf_op | source)
XLA Modules:
  0.0 196.3 jit_solution(5485446516036533210)
XLA Ops:
  0.0 1.3 copy.16.lam
  1.3 193.2 %layer.1 = bf16[384,512]{1,0:T(8,128)(2,1)} custom-call(bf16[384,2048]{1,0:T(8,128)(2,1)} %residual.1, bf16[384,128]{1,0:T(8,128)(2,1)} %qa.1, bf16[384,128]{1,0:T(8,128)(2,1)} %ka.1, bf16[384,128]{1,0:T(8,128)(2,1)} %va.1, bf16[384,256]{1,0:T(8,128)(2,1)} %qb.1, bf16[384,256]{1,0:T(8,128)(2,1)} %kb.1, bf16[384,128]{1,0:T(8,128)(2,1)} %vb.1, ...), custom_call_target="tpu_custom_call" | custom-call | tf_op jit(solution)/shard_map/layer/pallas_call | solution.py:438
  194.5 1.8 copy.18
where the time goes:
time: 197 us; the launch traced here: 196 us
  Pallas kernels  193 us (98%)
  local copies, waits for them, and re-layouts  3.06 us (2%)
    pallas_call x1, Pallas kernels, local(): pl.pallas_call(functools.partial(kernel, n, tp), out_shape=jax.ShapeDtype...  193 us

commit v1 on v0

v1 whole, which is shorter than its diff:
```python
import functools
import math

import jax
import jax.numpy as jnp
from jax import lax
from jax.experimental import pallas as pl
from jax.experimental.pallas import tpu as pltpu
from jax.sharding import PartitionSpec as P

eps_norm = 1e-06
head_scale = 0.8
MESH = pl.DeviceIdType.MESH
CHUNKS = 4
NT = (((1,), (1,)), ((), ()))


def flip(index, bit):
    return index + bit - 2 * bit * ((index // bit) % 2)


def flip_all(index, mask):
    bit = 1
    while bit <= mask:
        if mask & bit:
            index = flip(index, bit)
        bit *= 2
    return index


def kernel(
    n, tp, residual_in, qa, ka, va, qb, kb, vb, lam, gain, oa, ob, ngain, wg_in, wu_in, wd, out,
    kv_all, wg_turn, wu_turn, wg_all, wu_all, wd_all, out_all, heads_all, summed, normed, hidden, channel, near_out,
    near_in, far_out, far_in, mate_out, mate_in, mine, turned, residual, wg, wu, query_a, query_b, mix_out, mix, local_sem, twin_send, twin_recv, chain_send,
    kv_recv, cross_recv, cube_send, cube_recv, out_send, out_recv, head_send,
    head_recv, swap_sem, norm_send, norm_recv, red_send, red_recv,
):
    rows, width = residual.shape
    heads = lam.shape[1]
    sa, sb = qa.shape[1] // (2 * heads), qb.shape[1] // (2 * heads)
    vd = va.shape[1] // heads
    hv = heads * vd
    total = n * rows
    block = math.gcd(rows, 1 << min(7, ((1 << 19) // total).bit_length() - 1))
    nb = rows // block
    share = width // tp
    depth, units = wg.shape
    half = units // 2
    sp_me, tp_me = lax.axis_index("sp"), lax.axis_index("tp")
    line, length = sp_me // 2, n // 2
    core = tp_me % 2
    sp_twin, tp_twin = 2 * line + core, 2 * (tp_me // 2) + sp_me % 2
    apart = sp_me % 2 != core
    peers = [(tp_me + k) % tp for k in range(1, tp)]
    pair = n // 2
    side = (sp_me // pair) % 2
    mate = flip(sp_me, pair)
    bits = [pair]
    while bits[-1] > 1:
        bits.append(bits[-1] // 2)
    last = len(bits) - 1

    ck, cv = ka.shape[1], ka.shape[1] + kb.shape[1]
    part = rows // CHUNKS

    def strips(src, low, size):
        return [
            (src.at[pl.ds(c * part, part)], kv_all.at[sp_me, pl.ds(c * part, part), pl.ds(low, size)])
            for c in range(CHUNKS)
        ]

    pieces = [strips(ka, 0, ck), strips(kb, ck, kb.shape[1]), strips(va, cv, hv), strips(vb, cv + hv, hv)]
    swaps = [pieces[i][c] for c in range(CHUNKS) for i in range(4)]
    others = len(swaps)
    swaps += [(qa, query_a), (qb, query_b), (mix_out, mix), (mine, turned)]

    def twin(i):
        src, dst = swaps[i]
        return pltpu.make_async_remote_copy(
            src_ref=src, dst_ref=dst, send_sem=twin_send.at[i], recv_sem=twin_recv.at[i],
            device_id={"sp": sp_twin, "tp": tp_twin}, device_id_type=MESH,
        )

    def twin_local(i):
        src, dst = swaps[i]
        return pltpu.make_async_copy(src, dst, twin_recv.at[i])

    def twin_start(chosen):
        @pl.when(apart)
        def _():
            for i in chosen:
                twin(i).start()

        @pl.when(jnp.logical_not(apart))
        def _():
            for i in chosen:
                twin_local(i).start()

    def twin_wait(chosen):
        @pl.when(apart)
        def _():
            for i in chosen:
                twin(i).wait_recv()

        @pl.when(jnp.logical_not(apart))
        def _():
            for i in chosen:
                twin_local(i).wait()

    own = [
        (wg_in, wg),
        (wu_in, wu),
        (wd.at[pl.ds(pl.multiple_of(side * half, half), half)], wd_all.at[sp_me]),
        (oa, out_all.at[tp_me, pl.ds(0, hv)]),
        (ob, out_all.at[tp_me, pl.ds(hv, hv)]),
        (residual_in, residual),
    ]
    copies = [pltpu.make_async_copy(s, d, local_sem.at[i]) for i, (s, d) in enumerate(own)]
    for c in copies:
        c.start()

    barrier = pltpu.get_barrier_semaphore()
    for bit in bits:
        pl.semaphore_signal(barrier, inc=1, device_id={"sp": flip(sp_me, bit)}, device_id_type=MESH)
    for peer in peers:
        pl.semaphore_signal(barrier, inc=1, device_id={"tp": peer}, device_id_type=MESH)

    @pl.when(line > 0)
    def _():
        pl.semaphore_signal(barrier, inc=1, device_id={"sp": sp_me - 2}, device_id_type=MESH)

    @pl.when(line < length - 1)
    def _():
        pl.semaphore_signal(barrier, inc=1, device_id={"sp": sp_me + 2}, device_id_type=MESH)

    @pl.when(apart)
    def _():
        pl.semaphore_signal(
            barrier, inc=1, device_id={"sp": sp_twin, "tp": tp_twin}, device_id_type=MESH
        )

    for g in range(2):
        for h in range(heads):
            at = g * heads + h
            mix_out[at : at + 1, :] = jnp.full((1, mix_out.shape[1]), lam[g, h], jnp.float32)
    greeted = len(bits) + len(peers) + (line > 0).astype(jnp.int32) + (line < length - 1).astype(jnp.int32)
    pl.semaphore_wait(barrier, greeted + apart.astype(jnp.int32))

    towards = (sp_me + 2, sp_me - 2)

    def block_of(c, at, who):
        return kv_all.at[2 * at + who, pl.ds(c * part, part)]

    def chain(c, d, at):
        view = block_of(c, at, core)
        return pltpu.make_async_remote_copy(
            src_ref=view, dst_ref=view, send_sem=chain_send.at[c, d, at], recv_sem=kv_recv.at[c, at],
            device_id={"sp": towards[d]}, device_id_type=MESH,
        )

    def cross(c, at, arriving=False):
        view = block_of(c, at, 1 - core if arriving else core)
        return pltpu.make_async_remote_copy(
            src_ref=view, dst_ref=view, send_sem=chain_send.at[c, 2, at], recv_sem=cross_recv.at[c, at],
            device_id={"tp": flip(tp_me, 1)}, device_id_type=MESH,
        )

    rest = (line < length - 1, line > 0)

    def onward(c, d, at):
        @pl.when(rest[d])
        def _():
            chain(c, d, at).start()

    twin_start(range(others + 3))

    tp_bits = []
    while (tp >> (len(tp_bits) + 1)) > 0:
        tp_bits.append(tp >> (len(tp_bits) + 1))
    tp_order, tp_came = [0], {}
    for k, bit in enumerate(tp_bits):
        for held in list(tp_order):
            tp_came[held | bit] = (held, k)
            tp_order.append(held | bit)

    def tp_copy(gather, held, k, arriving):
        view, first, sends, recvs = gather
        mask = held | tp_bits[k]
        dst = view(flip_all(tp_me, mask if arriving else held))
        return pltpu.make_async_remote_copy(
            src_ref=first if first is not None and held == 0 and not arriving else dst, dst_ref=dst,
            send_sem=sends.at[mask - 1], recv_sem=recvs.at[mask - 1],
            device_id={"tp": flip(tp_me, tp_bits[k])}, device_id_type=MESH,
        )

    def tp_forward(gather, mask):
        for k in range(tp_came[mask][1] + 1 if mask else 0, len(tp_bits)):
            tp_copy(gather, mask, k, False).start()

    def tp_arrive(gather, masks):
        for mask in masks:
            held, k = tp_came[mask]
            tp_copy(gather, held, k, True).wait_recv()
            tp_forward(gather, mask)

    def tp_drain(gather):
        for mask in tp_order[1:]:
            held, k = tp_came[mask]
            tp_copy(gather, held, k, False).wait_send()

    out_gather = (lambda slot: out_all.at[slot], None, out_send, out_recv)
    head_gather = (lambda slot: heads_all.at[slot], turned, head_send, head_recv)
    for c in copies[:5]:
        c.wait()
    tp_forward(out_gather, 0)

    tile = math.gcd(units, 128)

    def turn(i):
        at = pl.ds(pl.multiple_of(i * tile, tile), tile)
        wg_turn[at, :] = wg[:, at].T
        wu_turn[at, :] = wu[:, at].T

    def turn_all(i, _):
        turn(i)
        return 0

    lax.fori_loop(0, units // tile, turn_all, 0)
    wg_all[sp_me] = wg_turn[pl.ds(pl.multiple_of(side * half, half), half), :]
    wu_all[sp_me] = wu_turn[pl.ds(pl.multiple_of(side * half, half), half), :]

    gathered = (wg_all, wu_all, wd_all)
    whole = (wg_turn, wu_turn, wd)

    def cube(a, held, k, arriving):
        mask = held | bits[k]
        owner = flip_all(sp_me, mask if arriving else held)
        dst = gathered[a].at[owner]
        src = dst
        if k == 0 and not arriving:
            src = whole[a].at[pl.ds(pl.multiple_of((1 - side) * half, half), half)]
        return pltpu.make_async_remote_copy(
            src_ref=src, dst_ref=dst,
            send_sem=cube_send.at[a, mask], recv_sem=cube_recv.at[a, mask],
            device_id={"sp": flip(sp_me, bits[k])}, device_id_type=MESH,
        )

    order = [0]
    came = {}
    for k, bit in enumerate(bits):
        for held in list(order):
            came[held | bit] = (held, k)
            order.append(held | bit)

    def forward(a, mask, least=0, most=len(bits)):
        first = came[mask][1] + 1 if mask else 0
        for k in range(max(first, least), most):
            cube(a, mask, k, False).start()

    def arrive(a, mask):
        held, k = came[mask]
        cube(a, held, k, True).wait_recv()
        forward(a, mask)

    events = []
    for k in range(len(bits)):
        for a in range(3):
            for mask in order[1:]:
                if came[mask][1] == k:
                    events.append((a, mask))

    def take(chosen):
        for a, mask in chosen:
            arrive(a, mask)
            events.remove((a, mask))

    def pick(a, low, high, paired=None):
        return [
            (b, mask) for b, mask in events
            if b == a and low <= came[mask][1] < high and (paired is None or bool(mask & pair) == paired)
        ]

    def own_rows_out():
        for a in (2, 0, 1):
            forward(a, 0, least=last)

    for c in range(CHUNKS):
        twin_wait(range(4 * c, 4 * c + 4))
        for d in range(2):
            onward(c, d, line)
        cross(c, line).start()

    @pl.when(apart)
    def _():
        own_rows_out()

    forward(0, 0, least=1, most=last)
    outer = jnp.logical_or(line < length // 4, line >= length - length // 4)

    def to_mate(chosen, where):
        @pl.when(where)
        def _():
            for a in chosen:
                forward(a, 0, most=1)

    to_mate([0], outer)
    for t in range(1, length):
        for d in range(2):
            at = line - t if d == 0 else line + t

            @pl.when(at >= 0 if d == 0 else at < length)
            def _():
                for c in range(CHUNKS):
                    chain(c, d, at).wait_recv()
                    onward(c, d, at)
                    cross(c, at).start()

        if t == 1:
            @pl.when(jnp.logical_not(apart))
            def _():
                own_rows_out()

        if t <= 2:
            to_mate([t], outer)
        if t == min(2, length - 1):
            take(pick(0, 1, last, False))
    for a in (1, 2):
        forward(a, 0, least=1, most=last)
    twin_wait(range(others, others + 3))
    for c in range(CHUNKS):
        for at in range(length):
            cross(c, at, True).wait_recv()

    def attend(group, r):
        queries = query_a if group == 0 else query_b
        size = sa if group == 0 else sb
        base = 0 if group == 0 else ck
        factor = size ** (-0.5) * math.log2(math.e)
        at = pl.ds(pl.multiple_of(r * block, block), block)
        for h in range(heads):
            start = 2 * h * size
            query = queries[at, start : start + 2 * size]
            value = kv_all[:, :, cv + group * hv + h * vd : cv + group * hv + (h + 1) * vd].reshape(total, vd)
            lanes = lax.broadcasted_iota(jnp.int32, query.shape, 1)
            ratios = []
            for j in range(2):
                if size % 128 == 0:
                    q = query[:, j * size : (j + 1) * size]
                    low = base + start + j * size
                    key = kv_all[:, :, low : low + size].reshape(total, size)
                else:
                    q = jnp.where(lanes // size == j, query, jnp.zeros_like(query))
                    low = base + start
                    key = kv_all[:, :, low : low + 2 * size].reshape(total, 2 * size)
                scores = lax.dot_general(q, key, NT, preferred_element_type=jnp.float32)
                peak = jnp.max(scores, axis=1, keepdims=True)
                weights = jnp.exp2((scores - peak) * factor)
                denom = jnp.sum(weights, axis=1, keepdims=True)
                numer = jnp.dot(weights.astype(jnp.bfloat16), value, preferred_element_type=jnp.float32)
                ratios.append(numer / denom)
            mixed = ratios[0] - mix[group * heads + h : group * heads + h + 1, :vd] * ratios[1]
            inverse = lax.rsqrt(jnp.mean(mixed * mixed, axis=-1, keepdims=True) + eps_norm)
            result = mixed * inverse * gain[group : group + 1, :] * head_scale
            col = group * hv + h * vd
            mine[at, col : col + vd] = result.astype(jnp.bfloat16)

    for group in range(2):
        def body(r, _, group=group):
            attend(group, r)
            return 0

        lax.fori_loop(0, nb, body, 0)
        if group == 0:
            tp_arrive(out_gather, tp_order[1:-1])

    twin_start([others + 3])
    take(pick(1, 1, last, False))
    to_mate(range(3), jnp.logical_not(outer))
    tp_arrive(out_gather, tp_order[-1:])
    twin_wait([others + 3])
    tp_forward(head_gather, 0)
    take(pick(0, 0, 1))
    take(pick(2, 1, last, False))
    tp_arrive(head_gather, tp_order[1:])
    heads_all[tp_me] = turned[...]

    tall = math.gcd(rows, 128)
    count = rows // tall

    def swap(r, arriving):
        there = 1 - side if arriving else side
        view = normed.at[there, tp_me, pl.ds(pl.multiple_of(r * tall, tall), tall)]
        return pltpu.make_async_remote_copy(
            src_ref=view, dst_ref=view, send_sem=swap_sem.at[0, r], recv_sem=swap_sem.at[1, r],
            device_id={"sp": mate}, device_id_type=MESH,
        )

    def project(r, _):
        @pl.when(r > 0)
        def _():
            swap(r - 1, False).start()

        at = pl.ds(pl.multiple_of(r * tall, tall), tall)
        acc = residual[at, :].astype(jnp.float32)
        for d in range(tp):
            acc = acc + jnp.dot(heads_all[d, at, :], out_all[d], preferred_element_type=jnp.float32)
        inverse = lax.rsqrt(jnp.mean(acc * acc, axis=-1, keepdims=True) + eps_norm)
        scaled = (acc * inverse * ngain[...]).astype(jnp.bfloat16)
        for d in range(tp):
            normed[side, d, at, :] = scaled[:, d * share : (d + 1) * share]

            @pl.when(d == tp_me)
            def _():
                summed[at, :] = acc[:, d * share : (d + 1) * share]

        return 0

    copies[5].wait()
    lax.fori_loop(0, count, project, 0)
    swap(count - 1, False).start()
    norm_gathers = [
        (
            lambda slot, r=r: normed.at[1 - side, slot, pl.ds(r * tall, tall)], None,
            norm_send.at[r], norm_recv.at[r],
        )
        for r in range(count)
    ]
    take(pick(1, 0, 1))
    take(pick(0, 1, last))
    for r in range(count):
        swap(r, True).wait_recv()
        tp_forward(norm_gathers[r], 0)
    take(pick(1, 1, last))
    take(pick(2, 0, 1))
    take(pick(0, last, last + 1))
    take(pick(1, last, last + 1))

    step_cols = share // depth

    def feed(where):
        gate = jnp.zeros((rows, half), jnp.float32)
        upward = jnp.zeros((rows, half), jnp.float32)
        for s in range(n):
            low = (s % step_cols) * depth
            x = normed[where, s // step_cols, :, low : low + depth]
            gate = gate + lax.dot_general(x, wg_all[s], NT, preferred_element_type=jnp.float32)
            upward = upward + lax.dot_general(x, wu_all[s], NT, preferred_element_type=jnp.float32)
        hidden[where] = (gate / (1.0 + jnp.exp(-gate)) * upward).astype(jnp.bfloat16)

    def feed_one(i, _):
        @pl.when(i == 1)
        def _():
            for r in range(count):
                tp_arrive(norm_gathers[r], tp_order[1:])

        feed((side + i) % 2)
        return 0

    lax.fori_loop(0, 2, feed_one, 0)
    cols = wd_all.shape[2]
    ratio = share // cols
    east = tp_me // 2

    def hand(src, dst, group, index, **target):
        return pltpu.make_async_remote_copy(
            src_ref=src, dst_ref=dst, send_sem=red_send.at[group, index], recv_sem=red_recv.at[group, index],
            device_id=target, device_id_type=MESH,
        )

    def near(index):
        return hand(near_out.at[index], near_in.at[index], 0, index, tp=flip(tp_me, 1))

    def far(index):
        return hand(far_out.at[index], far_in.at[index], 1, index, tp=flip(tp_me, 2))

    def across(index):
        return hand(mate_out.at[index], mate_in.at[index], 2, index, sp=mate)

    def slab_of(mask):
        slab = flip_all(sp_me, mask)
        target = slab // ratio
        return slab, target, (target // 2) * ratio + slab % ratio, slab % ratio

    def product(where, slab):
        return jnp.dot(hidden[where], wd_all[slab], preferred_element_type=jnp.float32)

    def give(mask):
        slab, target, index, _ = slab_of(mask)

        @pl.when(target % 2 != core)
        def _():
            def one(where, _):
                near_out[index, where] = product(where, slab).astype(jnp.bfloat16)
                return 0

            lax.fori_loop(0, 2, one, 0)
            near(index).start()

    def gain_near(mask):
        slab, target, index, low = slab_of(mask)

        @pl.when(target % 2 == core)
        def _():
            near(index).wait_recv()

            @pl.when(target // 2 == east)
            def _():
                def one(where, _):
                    channel[low, where] = product(where, slab) + near_in[index, where].astype(jnp.float32)
                    return 0

                lax.fori_loop(0, 2, one, 0)

            @pl.when(target // 2 != east)
            def _():
                def one(where, _):
                    both = product(where, slab) + near_in[index, where].astype(jnp.float32)
                    far_out[low, where] = both.astype(jnp.bfloat16)
                    return 0

                lax.fori_loop(0, 2, one, 0)
                far(low).start()

    def gain_far(mask):
        slab, target, index, low = slab_of(mask)

        @pl.when(target == tp_me)
        def _():
            far(low).wait_recv()
            channel[low, 1 - side] = channel[low, 1 - side] + far_in[low, 1 - side].astype(jnp.float32)
            mate_out[low] = channel[low, 1 - side].astype(jnp.bfloat16)
            across(low).start()
            channel[low, side] = channel[low, side] + far_in[low, side].astype(jnp.float32)

    steps = [m ^ p for m in order if not m & pair for p in (0, pair)]
    for i in range(len(steps) + 2):
        if i < len(steps):
            held = steps[i]
            if i == 0:
                take(pick(2, 1, last))
            take([e for e in events if e[1] == held])
            give(held)
        if 0 <= i - 1 < len(steps):
            gain_near(steps[i - 1])
        if 0 <= i - 2 < len(steps):
            gain_far(steps[i - 2])
    for low in range(ratio):
        across(low).wait_recv()
        final = channel[low, side] + mate_in[low].astype(jnp.float32)
        at = slice(low * cols, (low + 1) * cols)
        out[:, at] = (summed[:, at] + 0.5 * final).astype(jnp.bfloat16)

    for low in range(ratio):
        across(low).wait_send()
        far(low).wait_send()
    for index in range(n // 2):
        near(index).wait_send()
    for r in range(count):
        swap(r, False).wait_send()
    for gather in [out_gather, head_gather] + norm_gathers:
        tp_drain(gather)
    for a in range(3):
        for mask in order[1:]:
            held, k = came[mask]
            cube(a, held, k, False).wait_send()

    @pl.when(apart)
    def _():
        for i in range(len(swaps)):
            twin(i).wait_send()

    for c in range(CHUNKS):
        for at in range(length):
            cross(c, at).wait_send()
            for d in range(2):
                @pl.when(jnp.logical_and(rest[d], at <= line if d == 0 else at >= line))
                def _():
                    chain(c, d, at).wait_send()


def local(
    n, tp, residual, queries_a, keys_a, values_a, queries_b, keys_b, values_b, mix_lambda, head_gain,
    out_a, out_b, norm_gain, w_gate, w_up, w_down,
):
    rows, width = residual.shape
    share = width // tp
    units = w_gate.shape[1]
    hv = out_a.shape[0]
    cols = w_down.shape[1]
    tall = math.gcd(rows, 128)
    span = keys_a.shape[1] + keys_b.shape[1] + values_a.shape[1] + values_b.shape[1]
    vmem, anywhere = pl.BlockSpec(memory_space=pltpu.VMEM), pl.BlockSpec(memory_space=pl.ANY)
    smem = pl.BlockSpec(memory_space=pltpu.SMEM)
    bf16, f32 = jnp.bfloat16, jnp.float32
    dma = pltpu.SemaphoreType.DMA
    return pl.pallas_call(
        functools.partial(kernel, n, tp),
        out_shape=jax.ShapeDtypeStruct((rows, share), bf16),
        in_specs=[
            anywhere, anywhere, anywhere, anywhere, anywhere, anywhere, anywhere, smem, vmem,
            anywhere, anywhere, vmem, anywhere, anywhere, anywhere,
        ],
        out_specs=vmem,
        scratch_shapes=[
            pltpu.VMEM((n, rows, span), bf16),
            pltpu.VMEM((units, w_gate.shape[0]), bf16),
            pltpu.VMEM((units, w_gate.shape[0]), bf16),
            pltpu.VMEM((n, units // 2, w_gate.shape[0]), bf16),
            pltpu.VMEM((n, units // 2, w_gate.shape[0]), bf16),
            pltpu.VMEM((n, units // 2, w_down.shape[1]), bf16),
            pltpu.VMEM((tp, 2 * hv, width), bf16),
            pltpu.VMEM((tp, rows, 2 * hv), bf16),
            pltpu.VMEM((rows, share), f32),
            pltpu.VMEM((2, tp, rows, share), bf16),
            pltpu.VMEM((2, rows, units // 2), bf16),
            pltpu.VMEM((n // tp, 2, rows, cols), f32),
            pltpu.VMEM((n // 2, 2, rows, cols), bf16),
            pltpu.VMEM((n // 2, 2, rows, cols), bf16),
            pltpu.VMEM((n // tp, 2, rows, cols), bf16),
            pltpu.VMEM((n // tp, 2, rows, cols), bf16),
            pltpu.VMEM((n // tp, rows, cols), bf16),
            pltpu.VMEM((n // tp, rows, cols), bf16),
            pltpu.VMEM((rows, 2 * hv), bf16),
            pltpu.VMEM((rows, 2 * hv), bf16),
            pltpu.VMEM(residual.shape, bf16),
            pltpu.VMEM(w_gate.shape, bf16),
            pltpu.VMEM(w_up.shape, bf16),
            pltpu.VMEM(queries_a.shape, bf16),
            pltpu.VMEM(queries_b.shape, bf16),
            pltpu.VMEM((8 * -(-mix_lambda.size // 8), hv), f32),
            pltpu.VMEM((8 * -(-mix_lambda.size // 8), hv), f32),
            dma((6,)),
            dma((4 * CHUNKS + 4,)),
            dma((4 * CHUNKS + 4,)),
            dma((CHUNKS, 3, n // 2)),
            dma((CHUNKS, n // 2)),
            dma((CHUNKS, n // 2)),
            dma((3, n)),
            dma((3, n)),
            dma((tp - 1,)),
            dma((tp - 1,)),
            dma((tp - 1,)),
            dma((tp - 1,)),
            dma((2, rows // tall)),
            dma((rows // tall, tp - 1)),
            dma((rows // tall, tp - 1)),
            dma((3, n // 2)),
            dma((3, n // 2)),
        ],
        compiler_params=pltpu.CompilerParams(
            collective_id=0, has_side_effects=True, vmem_limit_bytes=63 * 1024 * 1024
        ),
        name="layer",
    )(
        residual, queries_a, keys_a, values_a, queries_b, keys_b, values_b, mix_lambda, head_gain,
        out_a, out_b, norm_gain.reshape(1, -1), w_gate, w_up, w_down,
    )


def solution(mesh):
    in_specs = (
        P("sp", None),
        P("sp", "tp"),
        P("sp", "tp"),
        P("sp", "tp"),
        P("sp", "tp"),
        P("sp", "tp"),
        P("sp", "tp"),
        P(None, "tp"),
        P(),
        P("tp", None),
        P("tp", None),
        P(),
        P("sp", "tp"),
        P("sp", "tp"),
        P("tp", "sp"),
    )
    body = functools.partial(local, mesh.shape["sp"], mesh.shape["tp"])
    return jax.shard_map(body, mesh=mesh, in_specs=in_specs, out_specs=P("sp", "tp"), check_vma=False)
```

time: 197 us -> 176 us (0.89)
  the two profiles are of different devices: /device:TPU:0 before, /device:TPU:10 now
where the time goes in v1:
time: 176 us
  Pallas kernels  173 us (98%)
  local copies, waits for them, and re-layouts  3.06 us (2%)
    pallas_call x1, Pallas kernels, local(): pl.pallas_call(functools.partial(kernel, n, tp), out_shape=jax.ShapeDtype...  173 us

profile of v1, /device:TPU:10, one launch (start us, length us, event | category | flops | bytes accessed | tf_op | source)
XLA Modules:
  0.0 176.2 jit_solution(13968543492066388158)
XLA Ops:
  0.0 1.3 copy.16.lam
  1.3 173.1 %layer.1 = bf16[384,512]{1,0:T(8,128)(2,1)} custom-call(bf16[384,2048]{1,0:T(8,128)(2,1)} %residual_in.1, bf16[384,128]{1,0:T(8,128)(2,1)} %qa.1, bf16[384,128]{1,0:T(8,128)(2,1)} %ka.1, bf16[384,128]{1,0:T(8,128)(2,1)} %va.1, bf16[384,256]{1,0:T(8,128)(2,1)} %qb.1, bf16[384,256]{1,0:T(8,128)(2,1)} %kb.1, bf16[384,128]{1,0:T(8,128)(2,1)} %vb.1, ...), custom_call_target="tpu_custom_call" | custom-call | tf_op jit(solution)/shard_map/layer/pallas_call | solution.py:596
  174.4 1.8 %copy.18 = bf16[384,512]{1,0:T(8,128)(2,1)} copy(bf16[384,512]{1,0:T(8,128)(2,1)} %layer.1) | data formatting | bytes 786432

commit v2 on v1

--- a/solution.py
+++ b/solution.py
@@ -31,7 +31,7 @@
 def kernel(
     n, tp, residual_in, qa, ka, va, qb, kb, vb, lam, gain, oa, ob, ngain, wg_in, wu_in, wd, out,
     kv_all, wg_turn, wu_turn, wg_all, wu_all, wd_all, out_all, heads_all, summed, normed, hidden, channel, near_out,
-    near_in, far_out, far_in, mate_out, mate_in, mine, turned, residual, wg, wu, query_a, query_b, mix_out, mix, local_sem, twin_send, twin_recv, chain_send,
+    near_in, far_out, far_in, mate_out, mate_in, mine, turned, residual, wg, wu, query_a, query_b, mix_out, mix, lend_send, lend_recv, local_sem, twin_send, twin_recv, chain_send,
     kv_recv, cross_recv, cube_send, cube_recv, out_send, out_recv, head_send,
     head_recv, swap_sem, norm_send, norm_recv, red_send, red_recv,
 ):
@@ -72,7 +72,7 @@
     pieces = [strips(ka, 0, ck), strips(kb, ck, kb.shape[1]), strips(va, cv, hv), strips(vb, cv + hv, hv)]
     swaps = [pieces[i][c] for c in range(CHUNKS) for i in range(4)]
     others = len(swaps)
-    swaps += [(qa, query_a), (qb, query_b), (mix_out, mix), (mine, turned)]
+    swaps += [(qa, query_a.at[0]), (qb, query_b.at[0]), (mix_out, mix), (mine.at[0], turned)]
 
     def twin(i):
         src, dst = swaps[i]
@@ -165,7 +165,20 @@
             device_id={"tp": flip(tp_me, 1)}, device_id_type=MESH,
         )
 
-    rest = (line < length - 1, line > 0)
+    quarter = length // 4
+    outer = jnp.logical_or(line < quarter, line >= length - quarter)
+    inner = jnp.logical_not(outer)
+    rest = (line + 1 < length - quarter, line - 1 >= quarter)
+    reach = (line < length - quarter, line >= quarter)
+    lender = flip(sp_me, n // 4)
+    loans = [(query_a.at[0], query_a.at[1]), (query_b.at[0], query_b.at[1]), (mine.at[1], mine.at[0])]
+
+    def lend(i):
+        src, dst = loans[i]
+        return pltpu.make_async_remote_copy(
+            src_ref=src, dst_ref=dst, send_sem=lend_send.at[i], recv_sem=lend_recv.at[i],
+            device_id={"sp": lender}, device_id_type=MESH,
+        )
 
     def onward(c, d, at):
         @pl.when(rest[d])
@@ -284,55 +297,68 @@
         for a in (2, 0, 1):
             forward(a, 0, least=last)
 
+    def over(c, at):
+        @pl.when(inner)
+        def _():
+            cross(c, at).start()
+
+    def to_mate(chosen, where):
+        @pl.when(where)
+        def _():
+            for a in chosen:
+                forward(a, 0, most=1)
+
     for c in range(CHUNKS):
         twin_wait(range(4 * c, 4 * c + 4))
         for d in range(2):
             onward(c, d, line)
-        cross(c, line).start()
+        over(c, line)
 
     @pl.when(apart)
     def _():
         own_rows_out()
 
     forward(0, 0, least=1, most=last)
-    outer = jnp.logical_or(line < length // 4, line >= length - length // 4)
-
-    def to_mate(chosen, where):
-        @pl.when(where)
-        def _():
-            for a in chosen:
-                forward(a, 0, most=1)
+    twin_wait(range(others, others + 3))
+
+    @pl.when(outer)
+    def _():
+        lend(0).start()
+        lend(1).start()
 
     to_mate([0], outer)
     for t in range(1, length):
         for d in range(2):
             at = line - t if d == 0 else line + t
 
-            @pl.when(at >= 0 if d == 0 else at < length)
+            @pl.when(jnp.logical_and(reach[d], at >= 0 if d == 0 else at < length))
             def _():
                 for c in range(CHUNKS):
                     chain(c, d, at).wait_recv()
                     onward(c, d, at)
-                    cross(c, at).start()
+                    over(c, at)
 
         if t == 1:
             @pl.when(jnp.logical_not(apart))
             def _():
                 own_rows_out()
 
-        if t <= 2:
-            to_mate([t], outer)
-        if t == min(2, length - 1):
-            take(pick(0, 1, last, False))
-    for a in (1, 2):
-        forward(a, 0, least=1, most=last)
-    twin_wait(range(others, others + 3))
-    for c in range(CHUNKS):
-        for at in range(length):
-            cross(c, at, True).wait_recv()
-
-    def attend(group, r):
-        queries = query_a if group == 0 else query_b
+    take(pick(0, 1, last, False))
+    to_mate([0], inner)
+    forward(1, 0, least=1, most=last)
+    to_mate([1], outer)
+    to_mate([1], inner)
+
+    @pl.when(inner)
+    def _():
+        for c in range(CHUNKS):
+            for at in range(length):
+                cross(c, at, True).wait_recv()
+        lend(0).wait_recv()
+        lend(1).wait_recv()
+
+    def attend(which, group, r):
+        queries = query_a.at[which] if group == 0 else query_b.at[which]
         size = sa if group == 0 else sb
         base = 0 if group == 0 else ck
         factor = size ** (-0.5) * math.log2(math.e)
@@ -362,25 +388,36 @@
             inverse = lax.rsqrt(jnp.mean(mixed * mixed, axis=-1, keepdims=True) + eps_norm)
             result = mixed * inverse * gain[group : group + 1, :] * head_scale
             col = group * hv + h * vd
-            mine[at, col : col + vd] = result.astype(jnp.bfloat16)
-
-    for group in range(2):
-        def body(r, _, group=group):
-            attend(group, r)
-            return 0
-
-        lax.fori_loop(0, nb, body, 0)
-        if group == 0:
-            tp_arrive(out_gather, tp_order[1:-1])
+            mine[which, at, col : col + vd] = result.astype(jnp.bfloat16)
+
+    for which in (1, 0):
+        @pl.when(inner)
+        def _():
+            for group in range(2):
+                def body(r, _, group=group):
+                    attend(which, group, r)
+                    return 0
+
+                lax.fori_loop(0, nb, body, 0)
+            if which == 1:
+                lend(2).start()
+
+        if which == 1:
+            take(pick(0, 0, 1))
+            to_mate([2], outer)
+    take(pick(1, 1, last, False))
+
+    @pl.when(outer)
+    def _():
+        lend(2).wait_recv()
 
     twin_start([others + 3])
-    take(pick(1, 1, last, False))
-    to_mate(range(3), jnp.logical_not(outer))
-    tp_arrive(out_gather, tp_order[-1:])
     twin_wait([others + 3])
     tp_forward(head_gather, 0)
-    take(pick(0, 0, 1))
-    take(pick(2, 1, last, False))
+    tp_arrive(out_gather, tp_order[1:])
+    take(pick(1, 0, 1))
+    take(pick(0, 1, last))
+    forward(2, 0, least=1, most=last)
     tp_arrive(head_gather, tp_order[1:])
     heads_all[tp_me] = turned[...]
 
@@ -425,13 +462,12 @@
         )
         for r in range(count)
     ]
-    take(pick(1, 0, 1))
-    take(pick(0, 1, last))
+    take(pick(1, 1, last))
     for r in range(count):
         swap(r, True).wait_recv()
         tp_forward(norm_gathers[r], 0)
-    take(pick(1, 1, last))
-    take(pick(2, 0, 1))
+    to_mate([2], inner)
+    take(pick(2, 1, last, False))
     take(pick(0, last, last + 1))
     take(pick(1, last, last + 1))
 
@@ -452,6 +488,8 @@
         def _():
             for r in range(count):
                 tp_arrive(norm_gathers[r], tp_order[1:])
+            take(pick(2, 0, 1))
+            take(pick(2, 1, last))
 
         feed((side + i) % 2)
         return 0
@@ -470,80 +508,82 @@
     def near(index):
         return hand(near_out.at[index], near_in.at[index], 0, index, tp=flip(tp_me, 1))
 
-    def far(index):
-        return hand(far_out.at[index], far_in.at[index], 1, index, tp=flip(tp_me, 2))
+    def far(low, where):
+        return hand(far_out.at[low, where], far_in.at[low, where], 1, 2 * low + (where == side), tp=flip(tp_me, 2))
 
     def across(index):
         return hand(mate_out.at[index], mate_in.at[index], 2, index, sp=mate)
 
-    def slab_of(mask):
-        slab = flip_all(sp_me, mask)
-        target = slab // ratio
-        return slab, target, (target // 2) * ratio + slab % ratio, slab % ratio
-
     def product(where, slab):
         return jnp.dot(hidden[where], wd_all[slab], preferred_element_type=jnp.float32)
 
-    def give(mask):
-        slab, target, index, _ = slab_of(mask)
-
-        @pl.when(target % 2 != core)
-        def _():
-            def one(where, _):
-                near_out[index, where] = product(where, slab).astype(jnp.bfloat16)
-                return 0
-
-            lax.fori_loop(0, 2, one, 0)
-            near(index).start()
-
-    def gain_near(mask):
-        slab, target, index, low = slab_of(mask)
-
-        @pl.when(target % 2 == core)
-        def _():
-            near(index).wait_recv()
-
-            @pl.when(target // 2 == east)
-            def _():
-                def one(where, _):
-                    channel[low, where] = product(where, slab) + near_in[index, where].astype(jnp.float32)
-                    return 0
-
-                lax.fori_loop(0, 2, one, 0)
-
-            @pl.when(target // 2 != east)
-            def _():
-                def one(where, _):
-                    both = product(where, slab) + near_in[index, where].astype(jnp.float32)
-                    far_out[low, where] = both.astype(jnp.bfloat16)
-                    return 0
-
-                lax.fori_loop(0, 2, one, 0)
-                far(low).start()
-
-    def gain_far(mask):
-        slab, target, index, low = slab_of(mask)
-
-        @pl.when(target == tp_me)
-        def _():
-            far(low).wait_recv()
-            channel[low, 1 - side] = channel[low, 1 - side] + far_in[low, 1 - side].astype(jnp.float32)
-            mate_out[low] = channel[low, 1 - side].astype(jnp.bfloat16)
-            across(low).start()
-            channel[low, side] = channel[low, side] + far_in[low, side].astype(jnp.float32)
-
-    steps = [m ^ p for m in order if not m & pair for p in (0, pair)]
-    for i in range(len(steps) + 2):
-        if i < len(steps):
-            held = steps[i]
-            if i == 0:
-                take(pick(2, 1, last))
-            take([e for e in events if e[1] == held])
-            give(held)
-        if 0 <= i - 1 < len(steps):
-            gain_near(steps[i - 1])
-        if 0 <= i - 2 < len(steps):
-            gain_far(steps[i - 2])
+    late = flip_all(sp_me, n - 1)
+
+    def ready(slab):
+        @pl.when(slab == late)
+        def _():
+            for a, mask in events:
+                arrive(a, mask)
+
+    def give(to_east, low):
+        slab = (2 * to_east + 1 - core) * ratio + low
+        index = to_east * ratio + low
+        ready(slab)
+
+        def one(where, _):
+            near_out[index, where] = product(where, slab).astype(jnp.bfloat16)
+            return 0
+
+        lax.fori_loop(0, 2, one, 0)
+        near(index).start()
+
+    def relay(low):
+        slab = (2 * (1 - east) + core) * ratio + low
+        index = (1 - east) * ratio + low
+        ready(slab)
+        near(index).wait_recv()
+
+        def one(where, _):
+            both = product(where, slab) + near_in[index, where].astype(jnp.float32)
+            far_out[low, where] = both.astype(jnp.bfloat16)
+            return 0
+
+        lax.fori_loop(0, 2, one, 0)
+        far(low, 1 - side).start()
+        far(low, side).start()
+
+    def keep(low):
+        slab = tp_me * ratio + low
+        index = east * ratio + low
+        ready(slab)
+        near(index).wait_recv()
+
+        def one(where, _):
+            channel[low, where] = product(where, slab) + near_in[index, where].astype(jnp.float32)
+            return 0
+
+        lax.fori_loop(0, 2, one, 0)
+
+    take([e for e in events if e[1] != n - 1])
+
+    def reduce_one(i, _):
+        low = (late + 1 + i) % ratio
+        give(1 - east, low)
+        relay(low)
+        give(east, low)
+        keep(low)
+        return 0
+
+    lax.fori_loop(0, ratio, reduce_one, 0)
+    events.clear()
+    for i in range(ratio):
+        low = (late + 1 + i) % ratio
+        far(low, 1 - side).wait_recv()
+        both = channel[low, 1 - side] + far_in[low, 1 - side].astype(jnp.float32)
+        mate_out[low] = both.astype(jnp.bfloat16)
+        across(low).start()
+        far(low, side).wait_recv()
+        channel[low, side] = channel[low, side] + far_in[low, side].astype(jnp.float32)
     for low in range(ratio):
         across(low).wait_recv()
         final = channel[low, side] + mate_in[low].astype(jnp.float32)
@@ -552,7 +592,8 @@
 
     for low in range(ratio):
         across(low).wait_send()
-        far(low).wait_send()
+        for where in range(2):
+            far(low, where).wait_send()
     for index in range(n // 2):
         near(index).wait_send()
     for r in range(count):
@@ -569,9 +610,20 @@
         for i in range(len(swaps)):
             twin(i).wait_send()
 
+    @pl.when(outer)
+    def _():
+        lend(0).wait_send()
+        lend(1).wait_send()
+
+    @pl.when(inner)
+    def _():
+        lend(2).wait_send()
+        for c in range(CHUNKS):
+            for at in range(length):
+                cross(c, at).wait_send()
+
     for c in range(CHUNKS):
         for at in range(length):
-            cross(c, at).wait_send()
             for d in range(2):
                 @pl.when(jnp.logical_and(rest[d], at <= line if d == 0 else at >= line))
                 def _():
@@ -620,15 +672,17 @@
             pltpu.VMEM((n // tp, 2, rows, cols), bf16),
             pltpu.VMEM((n // tp, rows, cols), bf16),
             pltpu.VMEM((n // tp, rows, cols), bf16),
-            pltpu.VMEM((rows, 2 * hv), bf16),
+            pltpu.VMEM((2, rows, 2 * hv), bf16),
             pltpu.VMEM((rows, 2 * hv), bf16),
             pltpu.VMEM(residual.shape, bf16),
             pltpu.VMEM(w_gate.shape, bf16),
             pltpu.VMEM(w_up.shape, bf16),
-            pltpu.VMEM(queries_a.shape, bf16),
-            pltpu.VMEM(queries_b.shape, bf16),
+            pltpu.VMEM((2,) + queries_a.shape, bf16),
+            pltpu.VMEM((2,) + queries_b.shape, bf16),
             pltpu.VMEM((8 * -(-mix_lambda.size // 8), hv), f32),
             pltpu.VMEM((8 * -(-mix_lambda.size // 8), hv), f32),
+            dma((3,)),
+            dma((3,)),
             dma((6,)),
             dma((4 * CHUNKS + 4,)),
             dma((4 * CHUNKS + 4,)),

time: 176 us -> 154 us (0.88)
  the two profiles are of different devices: /device:TPU:10 before, /device:TPU:0 now
where the time goes in v2:
time: 154 us; the launch traced here: 153 us
  Pallas kernels  150 us (97%)
  local copies, waits for them, and re-layouts  3.06 us (2%)
    pallas_call x1, Pallas kernels, local(): pl.pallas_call(functools.partial(kernel, n, tp), out_shape=jax.ShapeDtype...  150 us

profile of v2, /device:TPU:0, one launch (start us, length us, event | category | flops | bytes accessed | tf_op | source)
XLA Modules:
  0.0 153.5 jit_solution(1735780447194333904)
XLA Ops:
  0.0 1.3 copy.16.lam
  1.3 150.4 %layer.1 = bf16[384,512]{1,0:T(8,128)(2,1)} custom-call(bf16[384,2048]{1,0:T(8,128)(2,1)} %residual_in.1, bf16[384,128]{1,0:T(8,128)(2,1)} %qa.1, bf16[384,128]{1,0:T(8,128)(2,1)} %ka.1, bf16[384,128]{1,0:T(8,128)(2,1)} %va.1, bf16[384,256]{1,0:T(8,128)(2,1)} %qb.1, bf16[384,256]{1,0:T(8,128)(2,1)} %kb.1, bf16[384,128]{1,0:T(8,128)(2,1)} %vb.1, ...), custom_call_target="tpu_custom_call" | custom-call | tf_op jit(solution)/shard_map/layer/pallas_call | solution.py:648
  151.7 1.8 %copy.18 = bf16[384,512]{1,0:T(8,128)(2,1)} copy(bf16[384,512]{1,0:T(8,128)(2,1)} %layer.1) | data formatting | bytes 786432
